TPU v7x, 32 devices: a whole 2x2x4 slice. The times are simulated.
32 devices in a mesh: sp: 8 (over z, x), tp: 4 (over y, core).
Axes of the slice: x: 2, y: 2, z: 4, core: 2. Of those that a mesh axis runs over, the one named last changes fastest.
Arguments:
- residual: bfloat16 [2048, 2048], P(('sp', 'tp')), may hold values from -6 to 6
- first_query: bfloat16 [2048, 512], P('sp', 'tp'), may hold values from -6 to 6
- second_query: bfloat16 [2048, 512], P('sp', 'tp'), may hold values from -6 to 6
- first_key: bfloat16 [2048, 512], P('sp', 'tp'), may hold values from -6 to 6
- second_key: bfloat16 [2048, 512], P('sp', 'tp'), may hold values from -6 to 6
- values: bfloat16 [2048, 1024], P('sp', 'tp'), may hold values from -6 to 6
- lambdas: float32 [8], P('tp'), may hold values from 0.3 to 0.8
- head_gain: float32 [128], replicated, may hold values from 0.1 to 1.9
- out_weight: bfloat16 [1024, 2048], P('tp'), may hold values from -0.1875 to 0.1875
- norm_gain: float32 [2048], replicated, may hold values from 0.1 to 1.9
- up_weight: bfloat16 [2048, 4096], P('sp', 'tp'), may hold values from -0.125 to 0.125
- down_weight: bfloat16 [4096, 2048], P('tp', 'sp'), may hold values from -0.09375 to 0.09375
Outputs:
- mixed: bfloat16 [2048, 2048], P(('sp', 'tp'))
All inputs are finite; a program needn't handle non-finite values.
Results may differ from a plain program's by a relative error of at most 0.019.
Values may be sent and summed in bfloat16 or wider, within the bound.
A program may use at most 128 MiB of HBM per device.

v0:
```python
import jax
import jax.numpy as jnp
from jax import lax
from jax.sharding import PartitionSpec as P


def rotate(blocked, positions):
    half = blocked.shape[-1] // 2
    inverse = 10000.0 ** (-jnp.arange(0, half, dtype=jnp.float32) * 2.0 / blocked.shape[-1])
    angle = positions[:, None] * inverse[None, :]
    cosine = jnp.cos(angle)[:, None, :]
    sine = jnp.sin(angle)[:, None, :]
    first, second = (blocked[..., :half], blocked[..., half:])
    return jnp.concatenate(
        [first * cosine - second * sine, second * cosine + first * sine], axis=-1
    )


def absorb(state, queries, keys, vals, factor):
    top, total, summed = state
    scores = jnp.einsum("qhe,khe->qhk", queries, keys, preferred_element_type=jnp.float32) * factor
    peak = jnp.maximum(top, jnp.max(scores, axis=-1))
    shrink = jnp.exp(top - peak)
    weights = jnp.exp(scores - peak[..., None])
    total = total * shrink + jnp.sum(weights, axis=-1)
    summed = summed * shrink[..., None] + jnp.einsum(
        "qhk,khe->qhe", weights.astype(jnp.bfloat16), vals, preferred_element_type=jnp.float32
    )
    return (peak, total, summed)


def layer_norm(stream, gain):
    center = stream - jnp.mean(stream, axis=-1, keepdims=True)
    spread = jnp.mean(center * center, axis=-1, keepdims=True)
    return center * lax.rsqrt(spread + 1e-05) * gain


def local(
    residual,
    first_query,
    second_query,
    first_key,
    second_key,
    values,
    lambdas,
    head_gain,
    out_weight,
    norm_gain,
    up_weight,
    down_weight,
):
    local_rows = first_query.shape[0]
    head_count = lambdas.shape[0]
    head_width = first_query.shape[1] // head_count
    value_width = values.shape[1] // head_count
    quarter_rows = local_rows // lax.axis_size("tp")
    factor = head_width ** (-0.5)
    positions = (lax.axis_index("sp") * local_rows + jnp.arange(local_rows)).astype(jnp.float32)

    def prepare(source):
        turned = rotate(
            source.astype(jnp.float32).reshape(local_rows, head_count, head_width), positions
        )
        return turned.astype(jnp.bfloat16)

    query_a, query_b = (prepare(first_query), prepare(second_query))
    key_a = prepare(first_key).reshape(local_rows, head_count * head_width)
    key_b = prepare(second_key).reshape(local_rows, head_count * head_width)
    start_state = (
        jnp.full((local_rows, head_count), -1e30, jnp.float32),
        jnp.zeros((local_rows, head_count), jnp.float32),
        jnp.zeros((local_rows, head_count, value_width), jnp.float32),
    )
    piece_a = lax.all_gather(key_a, "sp", axis=0, tiled=True)
    piece_b = lax.all_gather(key_b, "sp", axis=0, tiled=True)
    piece_v = lax.all_gather(values, "sp", axis=0, tiled=True)
    count = piece_a.shape[0]
    block = 512
    blocks = count // block

    def advance(state, item):
        block_a, block_b, block_v = item
        return (
            (
                absorb(state[0], query_a, block_a, block_v, factor),
                absorb(state[1], query_b, block_b, block_v, factor),
            ),
            None,
        )

    items = (
        piece_a.reshape(blocks, block, head_count, head_width),
        piece_b.reshape(blocks, block, head_count, head_width),
        piece_v.reshape(blocks, block, head_count, value_width),
    )
    state_a, state_b = lax.scan(advance, (start_state, start_state), items)[0]
    diff = state_a[2] / state_a[1][..., None] - lambdas[None, :, None] * (
        state_b[2] / state_b[1][..., None]
    )
    scale = lax.rsqrt(jnp.mean(diff * diff, axis=-1, keepdims=True) + 1e-05)
    flat = (
        (diff * scale * head_gain * 0.8)
        .astype(jnp.bfloat16)
        .reshape(local_rows, head_count * value_width)
    )
    projected = lax.psum(
        jnp.dot(flat, out_weight, preferred_element_type=jnp.float32).astype(jnp.bfloat16), "tp"
    ).astype(jnp.float32)
    stream = lax.all_gather(residual, "tp", axis=0, tiled=True)
    whole = layer_norm(stream.astype(jnp.float32) + projected, norm_gain).astype(jnp.bfloat16)
    own_normed = lax.dynamic_slice_in_dim(
        whole, lax.axis_index("tp") * quarter_rows, quarter_rows, 0
    )
    lifted = jnp.dot(
        whole,
        lax.all_gather(up_weight, "sp", axis=0, tiled=True),
        preferred_element_type=jnp.float32,
    )
    down_full = lax.all_gather(down_weight, "sp", axis=1, tiled=True)
    hidden = jnp.square(jax.nn.relu(lifted)).astype(jnp.bfloat16)
    lowered = lax.psum_scatter(
        jnp.dot(hidden, down_full, preferred_element_type=jnp.float32).astype(jnp.bfloat16),
        "tp",
        scatter_dimension=0,
        tiled=True,
    ).astype(jnp.float32)
    return (own_normed.astype(jnp.float32) + lowered).astype(jnp.bfloat16)


def solution(mesh):
    in_specs = (
        P(("sp", "tp"), None),
        P("sp", "tp"),
        P("sp", "tp"),
        P("sp", "tp"),
        P("sp", "tp"),
        P("sp", "tp"),
        P("tp"),
        P(),
        P("tp", None),
        P(),
        P("sp", "tp"),
        P("tp", "sp"),
    )
    out_specs = P(("sp", "tp"), None)
    return jax.shard_map(local, mesh=mesh, in_specs=in_specs, out_specs=out_specs, check_vma=False)
```

profile of v0, /device:TPU:0, one launch (start us, length us, event | category | flops | bytes accessed | tf_op | source)
XLA Modules:
  0.0 354.3 jit_solution(2607594345238030326)
XLA Ops:
  12.2 34.2 %all_gather.21 = bf16[2048,128]{0,1:T(8,128)(2,1)S(1)} all-gather(bf16[256,128]{0,1:T(8,128)(2,1)S(1)} %bitcast.66), channel_id=1, replica_groups=mesh['sp'=8,'tp'=4] {'sp'}, dimensions={0}, use_global_device_ids=true | all-gather | bytes 589824 | tf_op jit(solution)/shard_map/all_gather | solution.py:75
  47.7 31.6 %all_gather.19 = bf16[2048,128]{0,1:T(8,128)(2,1)S(1)} all-gather(bf16[256,128]{0,1:T(8,128)(2,1)S(1)} %bitcast.67), channel_id=1, replica_groups=mesh['sp'=8,'tp'=4] {'sp'}, dimensions={0}, use_global_device_ids=true | all-gather | bytes 589824 | tf_op jit(solution)/shard_map/all_gather | solution.py:74
  80.6 2.1 reshape.134
  82.7 42.6 %while.21 = (s32[]{:T(128)}, f32[256,2]{0,1:T(2,128)S(1)}, f32[256,2]{0,1:T(2,128)}, f32[256,2,128]{0,2,1:T(8,128)}, f32[256,2]{0,1:T(2,128)S(1)}, /*index=5*/f3...) while((s32[]{:T(128)}, f32[256,2]{0,1:T(2,128)S(1)}, ...), condition=%wide.region_5.6_spmd.clone, body=%wide.region_0.5_spmd.clone.sunk | while | flops 204870656 | bytes 9381043 | solution.py:96
  86.3 1.8 constant_dynamic-slice_fusion.2
  89.2 1.7 fusion.68
  94.9 1.3 fusion.66
  96.2 1.8 constant_dynamic-slice_fusion.2
  99.1 2.0 fusion.68
  101.1 2.0 fusion.67
  107.3 1.8 constant_dynamic-slice_fusion.2
  110.2 2.0 fusion.68
  112.2 2.0 fusion.67
  118.4 1.8 constant_dynamic-slice_fusion.2
  121.4 2.0 fusion.68
  123.4 2.0 fusion.67
  127.3 1.4 convolution_convert_fusion.1
  130.0 35.5 %all-reduce.2.cloned.1.call-done = bf16[256,2048]{1,0:T(8,128)(2,1)} async-done(((bf16[256,2048]{1,0:T(8,128)(2,1)}), bf16[256,2048]{1,0:T(8,128)(2,1)}) %all-reduce.2.cloned.1.call-update) | async-done | bytes 1048592 | tf_op jit(solution)/shard_map/psum | solution.py:106
  165.4 2.0 fusion.25
  168.5 74.0 %all-gather.11.cloned.1.call-done = bf16[1024,2048]{1,0:T(8,128)(2,1)} async-done(((bf16[1024,256]{1,0:T(8,128)(2,1)}), bf16[1024,2048]{1,0:T(8,128)(2,1)}) %all-gather.11.cloned.1.call-update) | async-done | bytes 4194320 | tf_op jit(solution)/shard_map/all_gather | solution.py:119
  242.5 73.0 %all-gather.9.cloned.1.call-done = bf16[2048,1024]{1,0:T(8,128)(2,1)} async-done(((bf16[256,1024]{1,0:T(8,128)(2,1)}), bf16[2048,1024]{1,0:T(8,128)(2,1)}) %all-gather.9.cloned.1.call-update) | async-done | bytes 4194320 | tf_op jit(solution)/shard_map/all_gather | solution.py:116
  315.5 6.8 %convolution_convert_fusion = bf16[256,2048]{1,0:T(8,128)(2,1)} fusion(bf16[1024,2048]{1,0:T(8,128)(2,1)} %all-gather.11.cloned.1.call-done, bf16[256,2048]{1,0:T(8,128)(2,1)S(1)} %multiply_convert_fusion, bf16[2048,1024]{1,0:T(8,128)(2,1)} %all-gather.9.cloned.1.call-done), kind=kOutput, calls=%fused_computation.37 | convolution fusion | flops 2148794368 | bytes 10485760 | tf_op jit(solution)/shard_map/dot_general | solution.py:122
  322.3 23.5 %reduce-scatter.2.cloned.1.call-done = bf16[64,2048]{1,0:T(8,128)(2,1)} async-done(((bf16[256,2048]{1,0:T(8,128)(2,1)}), bf16[64,2048]{1,0:T(8,128)(2,1)}) %reduce-scatter.2.cloned.1.call-update) | async-done | bytes 262160 | tf_op jit(solution)/shard_map/reduce_scatter | solution.py:121
  345.8 1.7 add_convert_fusion
  (98 shorter events, 32.5 us)
Async XLA Ops:
  6.5 120.7 %copy-start = (bf16[256,2048]{1,0:T(8,128)(2,1)S(1)}, bf16[256,2048]{1,0:T(8,128)(2,1)}, u32[]{:S(2)}) copy-start(bf16[256,2048]{1,0:T(8,128)(2,1)} %param.22) | copy-start | bytes 3145732
  6.5 74.1 %all-gather.7.cloned.1.call-start = ((), (), s32[]{:S(2)}) async-start(), calls=%async_computation.2 | async-start | bytes 1179648 | tf_op jit(solution)/shard_map/all_gather | solution.py:76
  7.3 122.7 %all-gather.5.cloned.1.call-start = ((), (), s32[]{:S(2)}) async-start(), calls=%async_computation.1 | async-start | bytes 1310720 | tf_op jit(solution)/shard_map/all_gather | solution.py:109
  8.0 157.4 %all-reduce.2.cloned.1.call-start = ((), (), s32[]{:S(2)}) async-start(), calls=%async_computation.3 | async-start | bytes 2097152 | tf_op jit(solution)/shard_map/psum | solution.py:106
  86.3 4.7 %copy-start.3 = (f32[256,2]{0,1:T(2,128)S(1)}, f32[256,2]{0,1:T(2,128)}, u32[]{:S(2)}) copy-start(f32[256,2]{0,1:T(2,128)} %get-tuple-element.265) | copy-start | bytes 6148 | tf_op jit(solution)/shard_map/while
  96.2 4.9 %copy-start.3 = (f32[256,2]{0,1:T(2,128)S(1)}, f32[256,2]{0,1:T(2,128)}, u32[]{:S(2)}) copy-start(f32[256,2]{0,1:T(2,128)} %get-tuple-element.265) | copy-start | bytes 6148 | tf_op jit(solution)/shard_map/while
  107.3 4.9 %copy-start.3 = (f32[256,2]{0,1:T(2,128)S(1)}, f32[256,2]{0,1:T(2,128)}, u32[]{:S(2)}) copy-start(f32[256,2]{0,1:T(2,128)} %get-tuple-element.265) | copy-start | bytes 6148 | tf_op jit(solution)/shard_map/while
  118.4 4.9 %copy-start.3 = (f32[256,2]{0,1:T(2,128)S(1)}, f32[256,2]{0,1:T(2,128)}, u32[]{:S(2)}) copy-start(f32[256,2]{0,1:T(2,128)} %get-tuple-element.265) | copy-start | bytes 6148 | tf_op jit(solution)/shard_map/while
  128.7 113.7 %all-gather.11.cloned.1.call-start = ((), (), s32[]{:S(2)}) async-start(), calls=%async_computation.5 | async-start | bytes 4718592 | tf_op jit(solution)/shard_map/all_gather | solution.py:119
  129.3 186.1 %all-gather.9.cloned.1.call-start = ((), (), s32[]{:S(2)}) async-start(), calls=%async_computation.4 | async-start | bytes 4718592 | tf_op jit(solution)/shard_map/all_gather | solution.py:116
  129.4 38.6 %copy-start.4 = (f32[2048]{0:T(1024)S(1)}, f32[2048]{0:T(1024)}, u32[]{:S(2)}) copy-start(f32[2048]{0:T(1024)} %param.23) | copy-start | bytes 24580
  129.9 215.9 %reduce-scatter.2.cloned.1.call-start = ((), (), s32[]{:S(2)}) async-start(), calls=%async_computation.6 | async-start | bytes 1310720 | tf_op jit(solution)/shard_map/reduce_scatter | solution.py:121
  130.0 37.5 %copy-start.1 = (bf16[256,2048]{1,0:T(8,128)(2,1)S(1)}, bf16[256,2048]{1,0:T(8,128)(2,1)}, u32[]{:S(2)}) copy-start(bf16[256,2048]{1,0:T(8,128)(2,1)} %all-gather.5.cloned.1.call-done) | copy-start | bytes 3145732
  165.4 2.0 copy-start.2
Sparse Core Ops, SparseCore 0:
  9.5 45.4 all-gather.6
  56.5 15.4 all-gather.4
  128.9 36.5 all-reduce.1
  167.3 75.0 all-gather.10
  244.4 70.9 all-gather.8
  322.4 23.2 reduce-scatter.1
where the time goes:
time: 355 us; the launch traced here: 354 us
  waiting for transfers between devices  208 us (59%)
  blocking collectives  65.8 us (19%)
  matrix products  33 us (9%)
  local copies, waits for them, and re-layouts  20.2 us (6%)
  between operations  13.7 us (4%)
  other arithmetic  12.9 us (4%)
    all_gather x1, waiting for transfers between devices, local(): down_full = lax.all_gather(down_weight, 'sp', axis=1, tiled=True)  74 us
    all_gather x1, waiting for transfers between devices, local(): lax.all_gather(up_weight, 'sp', axis=0, tiled=True)  73 us
    psum x1, waiting for transfers between devices, local(): lax.psum(jnp.dot(flat, out_weight, preferred_element_type=jnp.float32).as...  35.5 us
    all_gather x1, blocking collectives, local(): piece_b = lax.all_gather(key_b, 'sp', axis=0, tiled=True)  34.2 us
    all_gather x1, blocking collectives, local(): piece_a = lax.all_gather(key_a, 'sp', axis=0, tiled=True)  31.6 us
    reduce_scatter x1, waiting for transfers between devices, local(): lax.psum_scatter(jnp.dot(hidden, down_full, preferred_element_type=jnp.fl...  23.5 us
    dot_general x8, matrix products, absorb(): jnp.einsum('qhk,khe->qhe', weights.astype(jnp.bfloat16), vals, preferred_...  14.6 us
    dynamic_slice x8, local copies, waits for them, and re-layouts, local(): state_a, state_b = lax.scan(advance, (start_state, start_state), items)[0]  11.8 us
  transfers between devices with their start and end apart: 6, of which 4 were waited for; matrix products, arithmetic and copies ran while one was open for 16% of the time, Pallas kernels for 0%

commit v1 on v0

--- a/solution.py
+++ b/solution.py
@@ -71,8 +71,11 @@
         jnp.zeros((local_rows, head_count), jnp.float32),
         jnp.zeros((local_rows, head_count, value_width), jnp.float32),
     )
-    piece_a = lax.all_gather(key_a, "sp", axis=0, tiled=True)
-    piece_b = lax.all_gather(key_b, "sp", axis=0, tiled=True)
+    piece_a, piece_b = jnp.split(
+        lax.all_gather(jnp.concatenate([key_a, key_b], axis=1), "sp", axis=0, tiled=True),
+        [key_a.shape[1]],
+        axis=1,
+    )
     piece_v = lax.all_gather(values, "sp", axis=0, tiled=True)
     count = piece_a.shape[0]
     block = 512

time: 355 us -> 368 us (1.037)
  waiting for transfers between devices: 208 us -> 285 us
  blocking collectives: 65.8 us -> 0 us
    all_gather x2 -> x0, blocking collectives: 65.8 us -> none  [the longest x1 34.2 us: local(): piece_b = lax.all_gather(key_b, 'sp', axis=0, tiled=True)]
    all_gather x0 -> x1, waiting for transfers between devices: none -> 40.7 us  [local(): lax.all_gather(jnp.concatenate([key_a, key_b], axis=1), 'sp', axis=0, til...]
    all_gather x1, waiting for transfers between devices: 0.02 us -> 37.6 us  [local(): piece_v = lax.all_gather(values, 'sp', axis=0, tiled=True)]
  transfers between devices with their start and end apart: 6 -> 7, of which waited for: 4 -> 6; matrix products, arithmetic and copies ran while one was open for 16% -> 15% of each run, Pallas kernels for 0% -> 0%
where the time goes in v1:
time: 368 us; the launch traced here: 367 us
  waiting for transfers between devices  285 us (77%)
  matrix products  33 us (9%)
  local copies, waits for them, and re-layouts  21.7 us (6%)
  between operations  13.7 us (4%)
  other arithmetic  13.5 us (4%)
    all_gather x1, waiting for transfers between devices, local(): down_full = lax.all_gather(down_weight, 'sp', axis=1, tiled=True)  75.1 us
    all_gather x1, waiting for transfers between devices, local(): lax.all_gather(up_weight, 'sp', axis=0, tiled=True)  72.2 us
    all_gather x1, waiting for transfers between devices, local(): lax.all_gather(jnp.concatenate([key_a, key_b], axis=1), 'sp', axis=0, til...  40.7 us
    all_gather x1, waiting for transfers between devices, local(): piece_v = lax.all_gather(values, 'sp', axis=0, tiled=True)  37.6 us
    psum x1, waiting for transfers between devices, local(): lax.psum(jnp.dot(flat, out_weight, preferred_element_type=jnp.float32).as...  33.9 us
    reduce_scatter x1, waiting for transfers between devices, local(): lax.psum_scatter(jnp.dot(hidden, down_full, preferred_element_type=jnp.fl...  23.1 us
    dot_general x8, matrix products, absorb(): jnp.einsum('qhk,khe->qhe', weights.astype(jnp.bfloat16), vals, preferred_...  14.6 us
    dynamic_slice x8, local copies, waits for them, and re-layouts, local(): state_a, state_b = lax.scan(advance, (start_state, start_state), items)[0]  11.8 us
  transfers between devices with their start and end apart: 7, of which 6 were waited for; matrix products, arithmetic and copies ran while one was open for 15% of the time, Pallas kernels for 0%

profile of v1, /device:TPU:0, one launch (start us, length us, event | category | flops | bytes accessed | tf_op | source)
XLA Modules:
  0.0 367.4 jit_solution(14218933330201382051)
XLA Ops:
  13.0 40.7 %all-gather.8.cloned.1.call-done = bf16[2048,256]{0,1:T(8,128)(2,1)} async-done(((bf16[256,256]{0,1:T(8,128)(2,1)}), bf16[2048,256]{0,1:T(8,128)(2,1)}) %all-gather.8.cloned.1.call-update) | async-done | bytes 1048592 | tf_op jit(solution)/shard_map/all_gather | solution.py:75
  57.5 37.6 %all-gather.10.cloned.1.call-done = bf16[2048,256]{1,0:T(8,128)(2,1)} async-done(((bf16[256,256]{1,0:T(8,128)(2,1)}), bf16[2048,256]{1,0:T(8,128)(2,1)}) %all-gather.10.cloned.1.call-update) | async-done | bytes 1048592 | tf_op jit(solution)/shard_map/all_gather | solution.py:79
  95.1 2.1 reshape.136
  97.3 42.6 %while.21 = (s32[]{:T(128)}, f32[256,2]{0,1:T(2,128)S(1)}, f32[256,2]{0,1:T(2,128)}, f32[256,2,128]{0,2,1:T(8,128)}, f32[256,2]{0,1:T(2,128)S(1)}, /*index=5*/f3...) while((s32[]{:T(128)}, f32[256,2]{0,1:T(2,128)S(1)}, ...), condition=%wide.region_5.6_spmd.clone, body=%wide.region_0.5_spmd.clone.sunk | while | flops 204870656 | bytes 9381043 | solution.py:99
  100.8 1.8 constant_dynamic-slice_fusion.2
  103.8 1.7 fusion.69
  110.7 1.8 constant_dynamic-slice_fusion.2
  113.7 2.0 fusion.69
  115.7 2.0 fusion.68
  120.5 1.3 fusion.67
  121.8 1.8 constant_dynamic-slice_fusion.2
  124.8 2.0 fusion.69
  126.8 2.0 fusion.68
  133.0 1.8 constant_dynamic-slice_fusion.2
  135.9 2.0 fusion.69
  137.9 2.0 fusion.68
  141.8 1.4 convolution_convert_fusion.1
  144.6 33.9 %all-reduce.2.cloned.1.call-done = bf16[256,2048]{1,0:T(8,128)(2,1)} async-done(((bf16[256,2048]{1,0:T(8,128)(2,1)}), bf16[256,2048]{1,0:T(8,128)(2,1)}) %all-reduce.2.cloned.1.call-update) | async-done | bytes 1048592 | tf_op jit(solution)/shard_map/psum | solution.py:109
  178.4 2.0 fusion.25
  181.5 72.2 %all-gather.12.cloned.1.call-done = bf16[2048,1024]{1,0:T(8,128)(2,1)} async-done(((bf16[256,1024]{1,0:T(8,128)(2,1)}), bf16[2048,1024]{1,0:T(8,128)(2,1)}) %all-gather.12.cloned.1.call-update) | async-done | bytes 4194320 | tf_op jit(solution)/shard_map/all_gather | solution.py:119
  253.7 75.1 %all-gather.14.cloned.1.call-done = bf16[1024,2048]{1,0:T(8,128)(2,1)} async-done(((bf16[1024,256]{1,0:T(8,128)(2,1)}), bf16[1024,2048]{1,0:T(8,128)(2,1)}) %all-gather.14.cloned.1.call-update) | async-done | bytes 4194320 | tf_op jit(solution)/shard_map/all_gather | solution.py:122
  328.8 6.9 %convolution_convert_fusion = bf16[256,2048]{1,0:T(8,128)(2,1)} fusion(bf16[1024,2048]{1,0:T(8,128)(2,1)} %all-gather.14.cloned.1.call-done, bf16[256,2048]{1,0:T(8,128)(2,1)S(1)} %multiply_convert_fusion, bf16[2048,1024]{1,0:T(8,128)(2,1)} %all-gather.12.cloned.1.call-done), kind=kOutput, calls=%fused_computation.37 | convolution fusion | flops 2148794368 | bytes 10485760 | tf_op jit(solution)/shard_map/dot_general | solution.py:125
  335.7 23.1 %reduce-scatter.2.cloned.1.call-done = bf16[64,2048]{1,0:T(8,128)(2,1)} async-done(((bf16[256,2048]{1,0:T(8,128)(2,1)}), bf16[64,2048]{1,0:T(8,128)(2,1)}) %reduce-scatter.2.cloned.1.call-update) | async-done | bytes 262160 | tf_op jit(solution)/shard_map/reduce_scatter | solution.py:124
  358.8 1.7 add_convert_fusion
  (100 shorter events, 34.5 us)
Async XLA Ops:
  6.5 135.3 %copy-start = (bf16[256,2048]{1,0:T(8,128)(2,1)S(1)}, bf16[256,2048]{1,0:T(8,128)(2,1)}, u32[]{:S(2)}) copy-start(bf16[256,2048]{1,0:T(8,128)(2,1)} %param.22) | copy-start | bytes 3145732
  6.5 47.1 %all-gather.8.cloned.1.call-start = ((), (), s32[]{:S(2)}) async-start(), calls=%async_computation.2 | async-start | bytes 1179648 | tf_op jit(solution)/shard_map/all_gather | solution.py:75
  11.4 83.7 %all-gather.10.cloned.1.call-start = ((), (), s32[]{:S(2)}) async-start(), calls=%async_computation.3 | async-start | bytes 1179648 | tf_op jit(solution)/shard_map/all_gather | solution.py:79
  12.2 132.4 %all-gather.6.cloned.1.call-start = ((), (), s32[]{:S(2)}) async-start(), calls=%async_computation.1 | async-start | bytes 1310720 | tf_op jit(solution)/shard_map/all_gather | solution.py:112
  12.9 165.5 %all-reduce.2.cloned.1.call-start = ((), (), s32[]{:S(2)}) async-start(), calls=%async_computation.4 | async-start | bytes 2097152 | tf_op jit(solution)/shard_map/psum | solution.py:109
  100.8 4.7 %copy-start.3 = (f32[256,2]{0,1:T(2,128)S(1)}, f32[256,2]{0,1:T(2,128)}, u32[]{:S(2)}) copy-start(f32[256,2]{0,1:T(2,128)} %get-tuple-element.269) | copy-start | bytes 6148 | tf_op jit(solution)/shard_map/while
  110.7 5.0 %copy-start.3 = (f32[256,2]{0,1:T(2,128)S(1)}, f32[256,2]{0,1:T(2,128)}, u32[]{:S(2)}) copy-start(f32[256,2]{0,1:T(2,128)} %get-tuple-element.269) | copy-start | bytes 6148 | tf_op jit(solution)/shard_map/while
  121.8 5.0 %copy-start.3 = (f32[256,2]{0,1:T(2,128)S(1)}, f32[256,2]{0,1:T(2,128)}, u32[]{:S(2)}) copy-start(f32[256,2]{0,1:T(2,128)} %get-tuple-element.269) | copy-start | bytes 6148 | tf_op jit(solution)/shard_map/while
  133.0 5.0 %copy-start.3 = (f32[256,2]{0,1:T(2,128)S(1)}, f32[256,2]{0,1:T(2,128)}, u32[]{:S(2)}) copy-start(f32[256,2]{0,1:T(2,128)} %get-tuple-element.269) | copy-start | bytes 6148 | tf_op jit(solution)/shard_map/while
  143.3 110.4 %all-gather.12.cloned.1.call-start = ((), (), s32[]{:S(2)}) async-start(), calls=%async_computation.5 | async-start | bytes 4718592 | tf_op jit(solution)/shard_map/all_gather | solution.py:119
  143.9 184.9 %all-gather.14.cloned.1.call-start = ((), (), s32[]{:S(2)}) async-start(), calls=%async_computation.6 | async-start | bytes 4718592 | tf_op jit(solution)/shard_map/all_gather | solution.py:122
  143.9 37.0 %copy-start.4 = (f32[2048]{0:T(1024)S(1)}, f32[2048]{0:T(1024)}, u32[]{:S(2)}) copy-start(f32[2048]{0:T(1024)} %param.23) | copy-start | bytes 24580
  144.5 214.3 %reduce-scatter.2.cloned.1.call-start = ((), (), s32[]{:S(2)}) async-start(), calls=%async_computation.7 | async-start | bytes 1310720 | tf_op jit(solution)/shard_map/reduce_scatter | solution.py:124
  144.5 35.9 %copy-start.1 = (bf16[256,2048]{1,0:T(8,128)(2,1)S(1)}, bf16[256,2048]{1,0:T(8,128)(2,1)}, u32[]{:S(2)}) copy-start(bf16[256,2048]{1,0:T(8,128)(2,1)} %all-gather.6.cloned.1.call-done) | copy-start | bytes 3145732
  178.4 2.0 copy-start.2
Sparse Core Ops, SparseCore 0:
  11.5 42.1 all-gather.7
  55.8 39.2 all-gather.9
  96.7 15.4 all-gather.5
  143.4 34.9 all-reduce.1
  180.4 73.2 all-gather.11
  255.6 73.1 all-gather.13
  335.8 22.9 reduce-scatter.1
